TPU v7x, 32 devices: a whole 2x2x4 slice. The times are simulated.
32 devices in a mesh: sp: 8 (over z, y), tp: 4 (over x, core).
Axes of the slice: x: 2, y: 2, z: 4, core: 2. Of those that a mesh axis runs over, the one named last changes fastest.
Arguments:
- queries: bfloat16 [4096, 2048], P('sp', 'tp'), may hold values from -8 to 8
- keys: bfloat16 [4096, 512], P('sp', 'tp'), may hold values from -8 to 8
- values: bfloat16 [4096, 512], P('sp', 'tp'), may hold values from -6 to 6
- q_gain: float32 [128], replicated, may hold values from 0.1 to 5.8
- k_gain: float32 [128], replicated, may hold values from 0.1 to 5.8
- out_weight: bfloat16 [2048, 2048], replicated, may hold values from -0.125 to 0.125
- out_gain: float32 [2048], replicated, may hold values from 0.1 to 1.9
- residual_in: bfloat16 [4096, 2048], P(('sp', 'tp')), may hold values from -6 to 6
- mlp_gain: float32 [2048], replicated, may hold values from 0.1 to 1.9
- gate_weight: bfloat16 [2048, 5632], P('sp', 'tp'), may hold values from -0.125 to 0.125
- up_weight: bfloat16 [2048, 5632], P('sp', 'tp'), may hold values from -0.125 to 0.125
- down_weight: bfloat16 [5632, 2048], P('tp', 'sp'), may hold values from -0.078125 to 0.078125
- final_gain: float32 [2048], replicated, may hold values from 0.1 to 1.9
Outputs:
- layer_out: bfloat16 [4096, 2048], P(('sp', 'tp'))
All inputs are finite; a program needn't handle non-finite values.
Results may differ from a plain program's by a relative error of at most 0.015.
The roundings to bfloat16 on the way count: a program that leaves them out, or rounds other values in their place, can miss the bound.
Values may be sent and summed in bfloat16 or wider, within the bound.
A program may use at most 128 MiB of HBM per device.

v0:
```python
import math
import jax
import jax.numpy as jnp
from jax import lax
from jax.sharding import PartitionSpec as P

GRID_W = 64


def rms_scale(matrix):
    return matrix * lax.rsqrt(jnp.mean(matrix * matrix, axis=-1, keepdims=True) + 1e-06)


def rotary(matrix, positions):
    quarter = matrix.shape[-1] // 4
    freqs = 10000.0 ** (-jnp.arange(quarter, dtype=jnp.float32) / quarter)
    grid = jnp.stack([positions // GRID_W, positions % GRID_W], axis=-1).astype(jnp.float32)
    angle = grid[:, :, None] * freqs
    cosine = jnp.cos(angle)[:, None]
    sine = jnp.sin(angle)[:, None]
    parts = matrix.reshape(matrix.shape[:-1] + (2, 2, quarter))
    first = parts[..., 0, :]
    second = parts[..., 1, :]
    turned = jnp.stack([first * cosine - second * sine, second * cosine + first * sine], axis=-2)
    return turned.reshape(matrix.shape)


def on_device(
    queries,
    keys,
    values,
    q_gain,
    k_gain,
    out_weight,
    out_gain,
    residual_in,
    mlp_gain,
    gate_weight,
    up_weight,
    down_weight,
    final_gain,
):
    tok_rows = queries.shape[0]
    head_size = q_gain.shape[0]
    q_heads = queries.shape[1] // head_size
    kv_heads = keys.shape[1] // head_size
    group_size = q_heads // kv_heads
    positions = lax.axis_index("sp") * tok_rows + jnp.arange(tok_rows, dtype=jnp.int32)
    query_rot = rotary(
        rms_scale(queries.reshape(tok_rows, q_heads, head_size).astype(jnp.float32)) * q_gain,
        positions,
    ).astype(jnp.bfloat16)
    key_rot = rotary(
        rms_scale(keys.reshape(tok_rows, kv_heads, head_size).astype(jnp.float32)) * k_gain,
        positions,
    ).astype(jnp.bfloat16)
    key_flat = key_rot.reshape(tok_rows, kv_heads * head_size)
    grouped = query_rot.reshape(tok_rows, kv_heads, group_size, head_size)
    score_scale = head_size ** (-0.5)
    key_all, value_all = (
        lax.all_gather(key_flat, "sp", axis=0, tiled=True),
        lax.all_gather(values, "sp", axis=0, tiled=True),
    )
    total_rows = key_all.shape[0]
    span = math.gcd(total_rows, 1024)
    key_blocks = key_all.reshape(total_rows // span, span, kv_heads, head_size)
    value_blocks = value_all.reshape(total_rows // span, span, kv_heads, head_size)

    def step(run_state, blocks):
        highest, weight_sum, accum = run_state
        key_block, value_block = blocks
        scores = (
            jnp.einsum("qcgd,kcd->cgqk", grouped, key_block, preferred_element_type=jnp.float32)
            * score_scale
        )
        new_high = jnp.maximum(highest, jnp.max(scores, axis=-1))
        factor = jnp.exp(highest - new_high)
        exp_scores = jnp.exp(scores - new_high[..., None])
        weight_sum = weight_sum * factor + jnp.sum(exp_scores, axis=-1)
        accum = accum * factor[..., None] + jnp.einsum(
            "cgqk,kcd->cgqd",
            exp_scores.astype(jnp.bfloat16),
            value_block,
            preferred_element_type=jnp.float32,
        )
        return ((new_high, weight_sum, accum), None)

    start_state = (
        jnp.full((kv_heads, group_size, tok_rows), -1e30, jnp.float32),
        jnp.zeros((kv_heads, group_size, tok_rows), jnp.float32),
        jnp.zeros((kv_heads, group_size, tok_rows, head_size), jnp.float32),
    )
    final_state, unused = lax.scan(step, start_state, (key_blocks, value_blocks))
    highest, weight_sum, accum = final_state
    attended = (
        jnp.transpose(accum / weight_sum[..., None], (2, 0, 1, 3))
        .reshape(tok_rows, q_heads * head_size)
        .astype(jnp.bfloat16)
    )
    head_rows = lax.all_to_all(attended, "tp", split_axis=0, concat_axis=1, tiled=True)
    projected = jnp.dot(head_rows, out_weight, preferred_element_type=jnp.float32)
    mid_stream = (residual_in.astype(jnp.float32) + out_gain * rms_scale(projected)).astype(
        jnp.bfloat16
    )
    normed = (mlp_gain * rms_scale(mid_stream.astype(jnp.float32))).astype(jnp.bfloat16)
    mixer_in = lax.all_gather(normed, "tp", axis=0, tiled=True)
    gate_proj = jnp.dot(
        mixer_in,
        lax.all_gather(gate_weight, "sp", axis=0, tiled=True),
        preferred_element_type=jnp.float32,
    )
    up_proj = jnp.dot(
        mixer_in,
        lax.all_gather(up_weight, "sp", axis=0, tiled=True),
        preferred_element_type=jnp.float32,
    )
    down_full = lax.all_gather(down_weight, "sp", axis=1, tiled=True)
    hidden = (jax.nn.silu(gate_proj) * up_proj).astype(jnp.bfloat16)
    mlp_branch = lax.psum_scatter(
        jnp.dot(hidden, down_full, preferred_element_type=jnp.float32).astype(jnp.bfloat16),
        "tp",
        scatter_dimension=0,
        tiled=True,
    ).astype(jnp.float32)
    return (mid_stream.astype(jnp.float32) + final_gain * rms_scale(mlp_branch)).astype(
        jnp.bfloat16
    )


def solution(mesh):
    return jax.shard_map(
        on_device,
        mesh=mesh,
        in_specs=(
            P("sp", "tp"),
            P("sp", "tp"),
            P("sp", "tp"),
            P(),
            P(),
            P(),
            P(),
            P(("sp", "tp"), None),
            P(),
            P("sp", "tp"),
            P("sp", "tp"),
            P("tp", "sp"),
            P(),
        ),
        out_specs=P(("sp", "tp"), None),
        check_vma=False,
    )
```

profile of v0, /device:TPU:0, one launch (start us, length us, event | category | flops | bytes accessed | tf_op | source)
XLA Modules:
  0.0 513.3 jit_solution(11249257965567632647)
XLA Ops:
  6.6 1.0 copy.17
  7.7 0.7 fusion.33
  8.4 0.6 fusion.39
  9.0 0.7 pad_maximum_fusion.1
  9.7 0.7 all-gather.9.cloned.1.call-update
  10.5 1.3 copy.18
  11.8 0.7 mul.257
  12.7 0.5 multiply_cosine_fusion
  13.6 0.3 copy.20
  13.9 38.1 %all-gather.7.cloned.1.call-done = bf16[4096,128]{0,1:T(8,128)(2,1)} async-done(((bf16[512,128]{0,1:T(8,128)(2,1)}), bf16[4096,128]{0,1:T(8,128)(2,1)}) %all-gather.7.cloned.1.call-update) | async-done | bytes 1048592 | tf_op jit(solution)/shard_map/all_gather | solution.py:61
  52.0 1.6 copy.24
  53.6 39.8 %all-gather.9.cloned.1.call-done = bf16[4096,128]{1,0:T(8,128)(2,1)} async-done(((bf16[512,128]{1,0:T(8,128)(2,1)}), bf16[4096,128]{1,0:T(8,128)(2,1)}) %all-gather.9.cloned.1.call-update) | async-done | bytes 1048592 | tf_op jit(solution)/shard_map/all_gather | solution.py:62
  93.4 47.3 %while.15 = (s32[]{:T(128)}, f32[1,4,512]{2,1,0:T(4,128)S(1)}, f32[1,4,512]{2,1,0:T(4,128)S(1)}, f32[1,4,512,128]{3,2,1,0:T(8,128)S(1)}, bf16[4,1024,1,128]{3,1,...) while((s32[]{:T(128)}, f32[1,4,512]{2,1,0:T(4,128)S(1)}, ...), condition=%wide.region_5.6_spmd.clone, body=%wide.region_2.5_spmd.clone.sunk | while | flops 1091317760 | bytes 61997704 | solution.py:93
  93.4 4.5 bitcast_reduce_fusion.3
  97.9 4.6 fusion.60
  102.5 1.3 copy-done
  103.8 1.4 fusion.59
  105.2 4.5 bitcast_reduce_fusion.3
  109.7 4.6 fusion.60
  114.3 1.3 copy-done
  115.6 1.4 fusion.59
  117.0 4.5 bitcast_reduce_fusion.3
  121.5 4.6 fusion.60
  126.1 1.3 copy-done
  127.4 1.4 fusion.59
  128.9 4.5 bitcast_reduce_fusion.3
  133.4 4.6 fusion.60
  138.0 1.3 copy-done
  139.3 1.4 fusion.59
  140.7 0.3 fusion.31
  141.0 0.4 copy.21
  141.7 11.4 %all_to_all.16 = bf16[4,128,512]{2,1,0:T(8,128)(2,1)S(1)} all-to-all(bf16[4,128,512]{2,1,0:T(8,128)(2,1)S(1)} %convert_element_type.88), channel_id=1, replica_groups=mesh['sp'=8,'tp'=4] {'tp'}, dimensions={0} | all-to-all | bytes 1048576 | tf_op jit(solution)/shard_map/all_to_all | solution.py:100
  153.0 0.3 copy.22
  153.3 4.8 multiply_reduce_fusion
  158.1 0.4 fusion.27
  158.5 1.0 fusion.29
  159.6 0.5 all-gather.13.cloned.1.call-update
  160.2 0.5 all-gather.15.cloned.1.call-update
  160.8 0.5 all-gather.17.cloned.1.call-update
  161.5 18.5 %all-gather.11.cloned.1.call-done = bf16[512,2048]{1,0:T(8,128)(2,1)} async-done(((bf16[128,2048]{1,0:T(8,128)(2,1)}), bf16[512,2048]{1,0:T(8,128)(2,1)}) %all-gather.11.cloned.1.call-update) | async-done | bytes 2097168 | tf_op jit(solution)/shard_map/all_gather | solution.py:106
  180.1 94.4 %all-gather.13.cloned.1.call-done = bf16[2048,1408]{1,0:T(8,128)(2,1)} async-done(((bf16[256,1408]{1,0:T(8,128)(2,1)}), bf16[2048,1408]{1,0:T(8,128)(2,1)}) %all-gather.13.cloned.1.call-update) | async-done | bytes 5767184 | tf_op jit(solution)/shard_map/all_gather | solution.py:109
  274.4 8.2 %fusion.43 = f32[512,1408]{1,0:T(8,128)} fusion(bf16[512,2048]{1,0:T(8,128)(2,1)} %all-gather.11.cloned.1.call-done, bf16[2048,1408]{1,0:T(8,128)(2,1)} %all-gather.13.cloned.1.call-done), kind=kOutput, calls=%fused_computation.81 | convolution fusion | flops 2952790016 | bytes 10747904 | tf_op jit(solution)/shard_map/dot_general | solution.py:107
  282.7 84.3 %all-gather.15.cloned.1.call-done = bf16[2048,1408]{1,0:T(8,128)(2,1)} async-done(((bf16[256,1408]{1,0:T(8,128)(2,1)}), bf16[2048,1408]{1,0:T(8,128)(2,1)}) %all-gather.15.cloned.1.call-update) | async-done | bytes 5767184 | tf_op jit(solution)/shard_map/all_gather | solution.py:114
  367.0 93.2 %all-gather.17.cloned.1.call-done = bf16[1408,2048]{1,0:T(8,128)(2,1)} async-done(((bf16[1408,256]{1,0:T(8,128)(2,1)}), bf16[1408,2048]{1,0:T(8,128)(2,1)}) %all-gather.17.cloned.1.call-update) | async-done | bytes 5767184 | tf_op jit(solution)/shard_map/all_gather | solution.py:117
  460.2 13.3 %convolution_convert_fusion = bf16[512,2048]{1,0:T(8,128)(2,1)} fusion(bf16[1408,2048]{1,0:T(8,128)(2,1)} %all-gather.17.cloned.1.call-done, bf16[512,2048]{1,0:T(8,128)(2,1)S(1)} %copy-done.5, bf16[2048,1408]{1,0:T(8,128)(2,1)} %all-gather.15.cloned.1.call-done, f32[512,1408]{1,0:T(8,128)} %fusion.43), kind=kOutput, calls=%fused_computation.28 | convolution fusion | flops 5910953984 | bytes 18612224 | tf_op jit(solution)/shard_map/dot_general | solution.py:120
  473.6 29.5 %reduce-scatter.2.cloned.1.call-done = bf16[128,2048]{1,0:T(8,128)(2,1)} async-done(((bf16[512,2048]{1,0:T(8,128)(2,1)}), bf16[128,2048]{1,0:T(8,128)(2,1)}) %reduce-scatter.2.cloned.1.call-update) | async-done | bytes 524304 | tf_op jit(solution)/shard_map/reduce_scatter | solution.py:119
  503.1 1.2 fusion.25
  504.3 2.1 fusion.30
  (53 shorter events, 1.5 us)
Async XLA Ops:
  6.5 45.4 %all-gather.7.cloned.1.call-start = ((), (), s32[]{:S(2)}) async-start(), calls=%async_computation.2 | async-start | bytes 1179648 | tf_op jit(solution)/shard_map/all_gather | solution.py:61
  9.7 83.7 %all-gather.9.cloned.1.call-start = ((), (), s32[]{:S(2)}) async-start(), calls=%async_computation.3 | async-start | bytes 1179648 | tf_op jit(solution)/shard_map/all_gather | solution.py:62
  10.4 169.6 %all-gather.11.cloned.1.call-start = ((), (), s32[]{:S(2)}) async-start(), calls=%async_computation.4 | async-start | bytes 2621440 | tf_op jit(solution)/shard_map/all_gather | solution.py:106
  97.9 5.9 %copy-start = (f32[1024,512,4]{1,0,2:T(8,128)S(1)}, f32[1024,512,4]{1,0,2:T(8,128)}, u32[]{:S(2)}) copy-start(f32[1024,512,4]{1,0,2:T(8,128)} %get-tuple-element.155) | copy-start | bytes 25165828 | tf_op jit(solution)/shard_map/while
  109.7 5.9 %copy-start = (f32[1024,512,4]{1,0,2:T(8,128)S(1)}, f32[1024,512,4]{1,0,2:T(8,128)}, u32[]{:S(2)}) copy-start(f32[1024,512,4]{1,0,2:T(8,128)} %get-tuple-element.155) | copy-start | bytes 25165828 | tf_op jit(solution)/shard_map/while
  121.5 5.9 %copy-start = (f32[1024,512,4]{1,0,2:T(8,128)S(1)}, f32[1024,512,4]{1,0,2:T(8,128)}, u32[]{:S(2)}) copy-start(f32[1024,512,4]{1,0,2:T(8,128)} %get-tuple-element.155) | copy-start | bytes 25165828 | tf_op jit(solution)/shard_map/while
  133.3 5.9 %copy-start = (f32[1024,512,4]{1,0,2:T(8,128)S(1)}, f32[1024,512,4]{1,0,2:T(8,128)}, u32[]{:S(2)}) copy-start(f32[1024,512,4]{1,0,2:T(8,128)} %get-tuple-element.155) | copy-start | bytes 25165828 | tf_op jit(solution)/shard_map/while
  153.3 4.8 copy-start.1
  153.3 4.8 copy-start.2
  153.3 5.2 %copy-start.3 = (f32[2048]{0:T(1024)S(1)}, f32[2048]{0:T(1024)}, u32[]{:S(2)}) copy-start(f32[2048]{0:T(1024)} %param.23) | copy-start | bytes 24580
  159.5 114.9 %all-gather.13.cloned.1.call-start = ((), (), s32[]{:S(2)}) async-start(), calls=%async_computation.5 | async-start | bytes 6488064 | tf_op jit(solution)/shard_map/all_gather | solution.py:109
  160.1 206.9 %all-gather.15.cloned.1.call-start = ((), (), s32[]{:S(2)}) async-start(), calls=%async_computation.6 | async-start | bytes 6488064 | tf_op jit(solution)/shard_map/all_gather | solution.py:114
  160.7 299.5 %all-gather.17.cloned.1.call-start = ((), (), s32[]{:S(2)}) async-start(), calls=%async_computation.7 | async-start | bytes 6488064 | tf_op jit(solution)/shard_map/all_gather | solution.py:117
  161.3 341.8 %reduce-scatter.2.cloned.1.call-start = ((), (), s32[]{:S(2)}) async-start(), calls=%async_computation.8 | async-start | bytes 2621440 | tf_op jit(solution)/shard_map/reduce_scatter | solution.py:119
  180.1 280.2 %copy-start.5 = (bf16[512,2048]{1,0:T(8,128)(2,1)S(1)}, bf16[512,2048]{1,0:T(8,128)(2,1)}, u32[]{:S(2)}) copy-start(bf16[512,2048]{1,0:T(8,128)(2,1)} %all-gather.11.cloned.1.call-done) | copy-start | bytes 6291460
  282.7 221.7 %copy-start.4 = (f32[2048]{0:T(1024)S(1)}, f32[2048]{0:T(1024)}, u32[]{:S(2)}) copy-start(f32[2048]{0:T(1024)} %param.27) | copy-start | bytes 24580
Sparse Core Ops, SparseCore 0:
  9.8 42.1 all-gather.6
  54.1 39.2 all-gather.8
  159.7 20.3 all-gather.10
  182.1 92.3 all-gather.12
  276.5 90.4 all-gather.14
  368.9 91.2 all-gather.16
  473.7 29.3 reduce-scatter.1
where the time goes:
time: 514 us; the launch traced here: 513 us
  waiting for transfers between devices  400 us (78%)
  matrix products  62.7 us (12%)
  other arithmetic  13.9 us (3%)
  between operations  13.7 us (3%)
  blocking collectives  11.4 us (2%)
  local copies, waits for them, and re-layouts  11 us (2%)
    all_gather x1, waiting for transfers between devices, on_device(): lax.all_gather(gate_weight, 'sp', axis=0, tiled=True)  94.4 us
    all_gather x1, waiting for transfers between devices, on_device(): down_full = lax.all_gather(down_weight, 'sp', axis=1, tiled=True)  93.2 us
    all_gather x1, waiting for transfers between devices, on_device(): lax.all_gather(up_weight, 'sp', axis=0, tiled=True)  84.3 us
    all_gather x1, waiting for transfers between devices, on_device(): lax.all_gather(values, 'sp', axis=0, tiled=True)  39.8 us
    all_gather x1, waiting for transfers between devices, on_device(): lax.all_gather(key_flat, 'sp', axis=0, tiled=True)  38.1 us
    reduce_scatter x1, waiting for transfers between devices, on_device(): lax.psum_scatter(jnp.dot(hidden, down_full, preferred_element_type=jnp.fl...  29.5 us
    all_gather x1, waiting for transfers between devices, on_device(): mixer_in = lax.all_gather(normed, 'tp', axis=0, tiled=True)  18.5 us
    dot_general x4, matrix products, step(): jnp.einsum('cgqk,kcd->cgqd', exp_scores.astype(jnp.bfloat16), value_block...  18.4 us
  transfers between devices with their start and end apart: 7, of which 7 were waited for; matrix products, arithmetic and copies ran while one was open for 3% of the time, Pallas kernels for 0%

commit v1 on v0

--- a/solution.py
+++ b/solution.py
@@ -114,7 +114,7 @@
         lax.all_gather(up_weight, "sp", axis=0, tiled=True),
         preferred_element_type=jnp.float32,
     )
-    down_full = lax.all_gather(down_weight, "sp", axis=1, tiled=True)
+    down_full = jnp.concatenate(lax.all_gather(down_weight, "sp"), axis=1)
     hidden = (jax.nn.silu(gate_proj) * up_proj).astype(jnp.bfloat16)
     mlp_branch = lax.psum_scatter(
         jnp.dot(hidden, down_full, preferred_element_type=jnp.float32).astype(jnp.bfloat16),

time: 514 us -> 449 us (0.87)
  waiting for transfers between devices: 400 us -> 326 us
  local copies, waits for them, and re-layouts: 11 us -> 20 us
    all_gather x1, waiting for transfers between devices: 93.2 us -> 24.1 us  [on_device(): down_full = jnp.concatenate(lax.all_gather(down_weight, 'sp'), axis=1)]
    reshape x0 -> x1, local copies, waits for them, and re-layouts: none -> 8.32 us  [on_device(): down_full = jnp.concatenate(lax.all_gather(down_weight, 'sp'), axis=1)]
  transfers between devices with their start and end apart: 7 -> 7, of which waited for: 7 -> 7; matrix products, arithmetic and copies ran while one was open for 3% -> 16% of each run, Pallas kernels for 0% -> 0%
where the time goes in v1:
time: 449 us
  waiting for transfers between devices  326 us (73%)
  matrix products  63.4 us (14%)
  local copies, waits for them, and re-layouts  20 us (4%)
  other arithmetic  13.8 us (3%)
  between operations  13.7 us (3%)
  blocking collectives  11.4 us (3%)
    all_gather x1, waiting for transfers between devices, on_device(): lax.all_gather(gate_weight, 'sp', axis=0, tiled=True)  94.4 us
    all_gather x1, waiting for transfers between devices, on_device(): lax.all_gather(up_weight, 'sp', axis=0, tiled=True)  84.3 us
    all_gather x1, waiting for transfers between devices, on_device(): lax.all_gather(values, 'sp', axis=0, tiled=True)  39.8 us
    all_gather x1, waiting for transfers between devices, on_device(): lax.all_gather(key_flat, 'sp', axis=0, tiled=True)  37.3 us
    reduce_scatter x1, waiting for transfers between devices, on_device(): lax.psum_scatter(jnp.dot(hidden, down_full, preferred_element_type=jnp.fl...  29.5 us
    all_gather x1, waiting for transfers between devices, on_device(): down_full = jnp.concatenate(lax.all_gather(down_weight, 'sp'), axis=1)  24.1 us
    dot_general x4, matrix products, step(): jnp.einsum('cgqk,kcd->cgqd', exp_scores.astype(jnp.bfloat16), value_block...  18.8 us
    dot_general x4, matrix products, step(): jnp.einsum('qcgd,kcd->cgqk', grouped, key_block, preferred_element_type=j...  18.3 us
  transfers between devices with their start and end apart: 7, of which 7 were waited for; matrix products, arithmetic and copies ran while one was open for 16% of the time, Pallas kernels for 0%

profile of v1, /device:TPU:0, one launch (start us, length us, event | category | flops | bytes accessed | tf_op | source)
XLA Modules:
  0.0 448.8 jit_solution(11858819832367672950)
XLA Ops:
  6.6 1.0 copy.24
  7.7 0.7 fusion.33
  8.4 0.6 fusion.39
  9.0 0.7 pad_maximum_fusion.1
  9.7 0.7 all-gather.10.cloned.1.call-update
  10.5 0.7 all-gather.18.cloned.1.call-update
  11.2 0.5 multiply_cosine_fusion
  11.8 1.3 copy.25
  13.2 0.7 mul.257
  14.3 0.3 copy.27
  14.6 37.3 %all-gather.8.cloned.1.call-done = bf16[4096,128]{0,1:T(8,128)(2,1)} async-done(((bf16[512,128]{0,1:T(8,128)(2,1)}), bf16[4096,128]{0,1:T(8,128)(2,1)}) %all-gather.8.cloned.1.call-update) | async-done | bytes 1048592 | tf_op jit(solution)/shard_map/all_gather | solution.py:61
  52.0 1.6 copy.32
  53.6 39.8 %all-gather.10.cloned.1.call-done = bf16[4096,128]{1,0:T(8,128)(2,1)} async-done(((bf16[512,128]{1,0:T(8,128)(2,1)}), bf16[4096,128]{1,0:T(8,128)(2,1)}) %all-gather.10.cloned.1.call-update) | async-done | bytes 1048592 | tf_op jit(solution)/shard_map/all_gather | solution.py:62
  93.4 48.8 %while.15 = (s32[]{:T(128)}, f32[1,4,512]{2,1,0:T(4,128)S(1)}, f32[1,4,512]{2,1,0:T(4,128)S(1)}, f32[1,4,512,128]{3,2,1,0:T(8,128)S(1)}, bf16[4,1024,1,128]{3,1,...) while((s32[]{:T(128)}, f32[1,4,512]{2,1,0:T(4,128)S(1)}, ...), condition=%wide.region_5.6_spmd.clone, body=%wide.region_2.5_spmd.clone.sunk | while | flops 1091317760 | bytes 61997704 | solution.py:93
  93.4 4.6 %bitcast_reduce_fusion.3 = (f32[4,512]{1,0:T(4,128)S(1)}, f32[1024,512,4]{1,0,2:T(8,128)}) fusion(bf16[512,1,4,128]{3,0,2,1:T(8,128)(2,1)S(1)} %get-tuple-element.187, bf16[4,1024,1,128]{3,1,2,0:T(8,128)(2,1)S(1)} %get-tuple-element.186, s32[]{:T(128)} %get-tuple-element.173), kind=kOutput, calls=%fused_computation.1.clone.1 | convolution fusion | flops 541063168 | bytes 9183236 | tf_op jit(solution)/shard_map/while/body/eval_jaxpr/qcgd,kcd->cgqk/dot_general | solution.py:73
  98.0 4.7 %fusion.60 = f32[1,4,512,128]{3,2,1,0:T(8,128)S(1)} fusion(f32[1024,512,4]{1,0,2:T(8,128)} %get-tuple-element.162, f32[4,512]{1,0:T(4,128)S(1)} %bitcast.106, f32[1,4,512,128]{3,2,1,0:T(8,128)S(1)} %get-tuple-element.176, f32[4,512]{1,0:T(4,128)S(1)} %get-tuple-element.163, pred[]{:T(512)S(6)} %compare.22, ...), kind=kOutput, calls=%fused_computation.10.clone.1 | convolution fusion | flops 543948800 | bytes 10764801 | tf_op jit(solution)/shard_map/while/body/eval_jaxpr/cgqk,kcd->cgqd/dot_general | solution.py:80
  102.7 1.9 copy-done
  104.6 1.4 fusion.59
  106.1 4.6 %bitcast_reduce_fusion.3 = (f32[4,512]{1,0:T(4,128)S(1)}, f32[1024,512,4]{1,0,2:T(8,128)}) fusion(bf16[512,1,4,128]{3,0,2,1:T(8,128)(2,1)S(1)} %get-tuple-element.187, bf16[4,1024,1,128]{3,1,2,0:T(8,128)(2,1)S(1)} %get-tuple-element.186, s32[]{:T(128)} %get-tuple-element.173), kind=kOutput, calls=%fused_computation.1.clone.1 | convolution fusion | flops 541063168 | bytes 9183236 | tf_op jit(solution)/shard_map/while/body/eval_jaxpr/qcgd,kcd->cgqk/dot_general | solution.py:73
  110.6 4.6 %fusion.60 = f32[1,4,512,128]{3,2,1,0:T(8,128)S(1)} fusion(f32[1024,512,4]{1,0,2:T(8,128)} %get-tuple-element.162, f32[4,512]{1,0:T(4,128)S(1)} %bitcast.106, f32[1,4,512,128]{3,2,1,0:T(8,128)S(1)} %get-tuple-element.176, f32[4,512]{1,0:T(4,128)S(1)} %get-tuple-element.163, pred[]{:T(512)S(6)} %compare.22, ...), kind=kOutput, calls=%fused_computation.10.clone.1 | convolution fusion | flops 543948800 | bytes 10764801 | tf_op jit(solution)/shard_map/while/body/eval_jaxpr/cgqk,kcd->cgqd/dot_general | solution.py:80
  115.3 1.3 copy-done
  116.6 1.4 fusion.59
  118.0 4.6 %bitcast_reduce_fusion.3 = (f32[4,512]{1,0:T(4,128)S(1)}, f32[1024,512,4]{1,0,2:T(8,128)}) fusion(bf16[512,1,4,128]{3,0,2,1:T(8,128)(2,1)S(1)} %get-tuple-element.187, bf16[4,1024,1,128]{3,1,2,0:T(8,128)(2,1)S(1)} %get-tuple-element.186, s32[]{:T(128)} %get-tuple-element.173), kind=kOutput, calls=%fused_computation.1.clone.1 | convolution fusion | flops 541063168 | bytes 9183236 | tf_op jit(solution)/shard_map/while/body/eval_jaxpr/qcgd,kcd->cgqk/dot_general | solution.py:73
  122.6 4.6 %fusion.60 = f32[1,4,512,128]{3,2,1,0:T(8,128)S(1)} fusion(f32[1024,512,4]{1,0,2:T(8,128)} %get-tuple-element.162, f32[4,512]{1,0:T(4,128)S(1)} %bitcast.106, f32[1,4,512,128]{3,2,1,0:T(8,128)S(1)} %get-tuple-element.176, f32[4,512]{1,0:T(4,128)S(1)} %get-tuple-element.163, pred[]{:T(512)S(6)} %compare.22, ...), kind=kOutput, calls=%fused_computation.10.clone.1 | convolution fusion | flops 543948800 | bytes 10764801 | tf_op jit(solution)/shard_map/while/body/eval_jaxpr/cgqk,kcd->cgqd/dot_general | solution.py:80
  127.3 1.3 copy-done
  128.5 1.4 fusion.59
  130.0 4.6 %bitcast_reduce_fusion.3 = (f32[4,512]{1,0:T(4,128)S(1)}, f32[1024,512,4]{1,0,2:T(8,128)}) fusion(bf16[512,1,4,128]{3,0,2,1:T(8,128)(2,1)S(1)} %get-tuple-element.187, bf16[4,1024,1,128]{3,1,2,0:T(8,128)(2,1)S(1)} %get-tuple-element.186, s32[]{:T(128)} %get-tuple-element.173), kind=kOutput, calls=%fused_computation.1.clone.1 | convolution fusion | flops 541063168 | bytes 9183236 | tf_op jit(solution)/shard_map/while/body/eval_jaxpr/qcgd,kcd->cgqk/dot_general | solution.py:73
  134.6 4.8 %fusion.60 = f32[1,4,512,128]{3,2,1,0:T(8,128)S(1)} fusion(f32[1024,512,4]{1,0,2:T(8,128)} %get-tuple-element.162, f32[4,512]{1,0:T(4,128)S(1)} %bitcast.106, f32[1,4,512,128]{3,2,1,0:T(8,128)S(1)} %get-tuple-element.176, f32[4,512]{1,0:T(4,128)S(1)} %get-tuple-element.163, pred[]{:T(512)S(6)} %compare.22, ...), kind=kOutput, calls=%fused_computation.10.clone.1 | convolution fusion | flops 543948800 | bytes 10764801 | tf_op jit(solution)/shard_map/while/body/eval_jaxpr/cgqk,kcd->cgqd/dot_general | solution.py:80
  139.4 1.4 copy-done
  140.7 1.4 fusion.59
  142.2 0.3 fusion.31
  142.5 0.4 copy.28
  143.1 11.4 %all_to_all.16 = bf16[4,128,512]{2,1,0:T(8,128)(2,1)S(1)} all-to-all(bf16[4,128,512]{2,1,0:T(8,128)(2,1)S(1)} %convert_element_type.88), channel_id=1, replica_groups=mesh['sp'=8,'tp'=4] {'tp'}, dimensions={0} | all-to-all | bytes 1048576 | tf_op jit(solution)/shard_map/all_to_all | solution.py:100
  154.9 4.8 %multiply_reduce_fusion = (f32[128]{0:T(128)S(1)}, f32[128,2048]{1,0:T(8,128)S(1)}) fusion(bf16[128,2048]{0,1:T(8,128)(2,1)S(1)} %bitcast.109, bf16[2048,2048]{1,0:T(8,128)(2,1)} %param.20), kind=kOutput, calls=%fused_computation.42 | convolution fusion | flops 1074265984 | bytes 9961984 | tf_op jit(solution)/shard_map/dot_general | solution.py:101
  159.7 0.4 fusion.27
  160.1 1.0 fusion.29
  161.2 0.5 all-gather.14.cloned.1.call-update
  161.8 0.5 all-gather.16.cloned.1.call-update
  162.5 24.1 %all-gather.18.cloned.1.call-done = bf16[11264,256]{1,0:T(8,128)(2,1)} async-done(((bf16[1408,256]{1,0:T(8,128)(2,1)}), bf16[11264,256]{1,0:T(8,128)(2,1)}) %all-gather.18.cloned.1.call-update) | async-done | bytes 5767184 | tf_op jit(solution)/shard_map/all_gather | solution.py:117
  186.7 8.3 %copy.30 = bf16[1408,8,256]{0,2,1:T(8,128)(2,1)} copy(bf16[1408,8,256]{2,0,1:T(8,128)(2,1)} %bitcast.103) | data formatting | bytes 11534336 | tf_op jit(solution)/shard_map/reshape | solution.py:117
  195.0 13.9 %all-gather.12.cloned.1.call-done = bf16[512,2048]{1,0:T(8,128)(2,1)} async-done(((bf16[128,2048]{1,0:T(8,128)(2,1)}), bf16[512,2048]{1,0:T(8,128)(2,1)}) %all-gather.12.cloned.1.call-update) | async-done | bytes 2097168 | tf_op jit(solution)/shard_map/all_gather | solution.py:106
  208.8 94.4 %all-gather.14.cloned.1.call-done = bf16[2048,1408]{1,0:T(8,128)(2,1)} async-done(((bf16[256,1408]{1,0:T(8,128)(2,1)}), bf16[2048,1408]{1,0:T(8,128)(2,1)}) %all-gather.14.cloned.1.call-update) | async-done | bytes 5767184 | tf_op jit(solution)/shard_map/all_gather | solution.py:109
  303.2 8.3 %fusion.43 = f32[512,1408]{1,0:T(8,128)} fusion(bf16[512,2048]{1,0:T(8,128)(2,1)} %all-gather.12.cloned.1.call-done, bf16[2048,1408]{1,0:T(8,128)(2,1)} %all-gather.14.cloned.1.call-done), kind=kOutput, calls=%fused_computation.81 | convolution fusion | flops 2952790016 | bytes 10747904 | tf_op jit(solution)/shard_map/dot_general | solution.py:107
  311.5 84.3 %all-gather.16.cloned.1.call-done = bf16[2048,1408]{1,0:T(8,128)(2,1)} async-done(((bf16[256,1408]{1,0:T(8,128)(2,1)}), bf16[2048,1408]{1,0:T(8,128)(2,1)}) %all-gather.16.cloned.1.call-update) | async-done | bytes 5767184 | tf_op jit(solution)/shard_map/all_gather | solution.py:114
  395.8 13.3 %convolution_convert_fusion = bf16[512,2048]{1,0:T(8,128)(2,1)} fusion(bf16[1408,2048]{0,1:T(8,128)(2,1)} %bitcast.104, bf16[512,2048]{1,0:T(8,128)(2,1)S(1)} %copy-done.5, bf16[2048,1408]{1,0:T(8,128)(2,1)} %all-gather.16.cloned.1.call-done, f32[512,1408]{1,0:T(8,128)} %fusion.43), kind=kOutput, calls=%fused_computation.28 | convolution fusion | flops 5910953984 | bytes 18612224 | tf_op jit(solution)/shard_map/dot_general | solution.py:120
  409.1 29.5 %reduce-scatter.2.cloned.1.call-done = bf16[128,2048]{1,0:T(8,128)(2,1)} async-done(((bf16[512,2048]{1,0:T(8,128)(2,1)}), bf16[128,2048]{1,0:T(8,128)(2,1)}) %reduce-scatter.2.cloned.1.call-update) | async-done | bytes 524304 | tf_op jit(solution)/shard_map/reduce_scatter | solution.py:119
  438.6 1.2 fusion.25
  439.8 2.1 fusion.30
  (54 shorter events, 1.7 us)
Async XLA Ops:
  6.5 45.4 %all-gather.8.cloned.1.call-start = ((), (), s32[]{:S(2)}) async-start(), calls=%async_computation.2 | async-start | bytes 1179648 | tf_op jit(solution)/shard_map/all_gather | solution.py:61
  9.7 83.7 %all-gather.10.cloned.1.call-start = ((), (), s32[]{:S(2)}) async-start(), calls=%async_computation.3 | async-start | bytes 1179648 | tf_op jit(solution)/shard_map/all_gather | solution.py:62
  10.4 176.2 %all-gather.18.cloned.1.call-start = ((), (), s32[]{:S(2)}) async-start(), calls=%async_computation.8 | async-start | bytes 6488064 | tf_op jit(solution)/shard_map/all_gather | solution.py:117
  11.2 197.7 %all-gather.12.cloned.1.call-start = ((), (), s32[]{:S(2)}) async-start(), calls=%async_computation.4 | async-start | bytes 2621440 | tf_op jit(solution)/shard_map/all_gather | solution.py:106
  98.0 6.7 %copy-start = (f32[1024,512,4]{1,0,2:T(8,128)S(1)}, f32[1024,512,4]{1,0,2:T(8,128)}, u32[]{:S(2)}) copy-start(f32[1024,512,4]{1,0,2:T(8,128)} %get-tuple-element.162) | copy-start | bytes 25165828 | tf_op jit(solution)/shard_map/while
  110.6 6.0 %copy-start = (f32[1024,512,4]{1,0,2:T(8,128)S(1)}, f32[1024,512,4]{1,0,2:T(8,128)}, u32[]{:S(2)}) copy-start(f32[1024,512,4]{1,0,2:T(8,128)} %get-tuple-element.162) | copy-start | bytes 25165828 | tf_op jit(solution)/shard_map/while
  122.6 5.9 %copy-start = (f32[1024,512,4]{1,0,2:T(8,128)S(1)}, f32[1024,512,4]{1,0,2:T(8,128)}, u32[]{:S(2)}) copy-start(f32[1024,512,4]{1,0,2:T(8,128)} %get-tuple-element.162) | copy-start | bytes 25165828 | tf_op jit(solution)/shard_map/while
  134.5 6.2 %copy-start = (f32[1024,512,4]{1,0,2:T(8,128)S(1)}, f32[1024,512,4]{1,0,2:T(8,128)}, u32[]{:S(2)}) copy-start(f32[1024,512,4]{1,0,2:T(8,128)} %get-tuple-element.162) | copy-start | bytes 25165828 | tf_op jit(solution)/shard_map/while
  154.9 4.8 %copy-start.1 = (bf16[128,2048]{1,0:T(8,128)(2,1)S(1)}, bf16[128,2048]{1,0:T(8,128)(2,1)}, u32[]{:S(2)}) copy-start(bf16[128,2048]{1,0:T(8,128)(2,1)} %param.22) | copy-start | bytes 1572868
  154.9 4.8 %copy-start.2 = (f32[2048]{0:T(1024)S(1)}, f32[2048]{0:T(1024)}, u32[]{:S(2)}) copy-start(f32[2048]{0:T(1024)} %param.21) | copy-start | bytes 24580
  154.9 5.2 %copy-start.3 = (f32[2048]{0:T(1024)S(1)}, f32[2048]{0:T(1024)}, u32[]{:S(2)}) copy-start(f32[2048]{0:T(1024)} %param.23) | copy-start | bytes 24580
  161.1 142.1 %all-gather.14.cloned.1.call-start = ((), (), s32[]{:S(2)}) async-start(), calls=%async_computation.5 | async-start | bytes 6488064 | tf_op jit(solution)/shard_map/all_gather | solution.py:109
  161.7 234.1 %all-gather.16.cloned.1.call-start = ((), (), s32[]{:S(2)}) async-start(), calls=%async_computation.6 | async-start | bytes 6488064 | tf_op jit(solution)/shard_map/all_gather | solution.py:114
  162.3 276.3 %reduce-scatter.2.cloned.1.call-start = ((), (), s32[]{:S(2)}) async-start(), calls=%async_computation.7 | async-start | bytes 2621440 | tf_op jit(solution)/shard_map/reduce_scatter | solution.py:119
  208.8 186.9 %copy-start.5 = (bf16[512,2048]{1,0:T(8,128)(2,1)S(1)}, bf16[512,2048]{1,0:T(8,128)(2,1)}, u32[]{:S(2)}) copy-start(bf16[512,2048]{1,0:T(8,128)(2,1)} %all-gather.12.cloned.1.call-done) | copy-start | bytes 6291460
  395.8 44.1 %copy-start.4 = (f32[2048]{0:T(1024)S(1)}, f32[2048]{0:T(1024)}, u32[]{:S(2)}) copy-start(f32[2048]{0:T(1024)} %param.27) | copy-start | bytes 24580
Sparse Core Ops, SparseCore 0:
  9.8 42.1 all-gather.7
  54.1 39.2 all-gather.9
  95.6 91.0 all-gather.17
  188.1 20.7 all-gather.11
  210.9 92.3 all-gather.13
  305.3 90.4 all-gather.15
  409.2 29.3 reduce-scatter.1
